TPU v7x, 32 devices: a whole 2x2x4 slice. The times are simulated.
32 devices in a mesh: grp: 2 (over y), sp: 4 (over z), tp: 4 (over x, core).
Axes of the slice: x: 2, y: 2, z: 4, core: 2. Of those that a mesh axis runs over, the one named last changes fastest.
Arguments:
- resid: bfloat16 [5120, 2048], P(('grp', 'sp'), 'tp'), parts along dimension 0, may hold values from -6 to 6
- queries: bfloat16 [5120, 2048], P(('grp', 'sp'), 'tp'), parts along dimension 0, may hold values from -150 to 150
- keys_values: bfloat16 [5120, 8, 128], P(('grp', 'sp'), 'tp'), parts along dimension 0, may hold values from -4.5 to 4.5
- sink: float32 [32], P('tp'), may hold values from 3 to 7
- out_weight: bfloat16 [2048, 2048], P('tp'), may hold values from -2.390625 to 2.390625
- norm_gain: float32 [2048], replicated, may hold values from 0.1 to 1.9
- gate_weight: bfloat16 [2048, 5632], P('sp', 'tp'), may hold values from -0.125 to 0.125
- up_weight: bfloat16 [2048, 5632], P('sp', 'tp'), may hold values from -0.125 to 0.125
- down_weight: bfloat16 [5632, 2048], P('tp', 'sp'), may hold values from -0.078125 to 0.078125
Outputs:
- mixed: bfloat16 [5120, 2048], P(('grp', 'sp'), 'tp'), parts along dimension 0
There are 2 independent parts, one for each index of `grp`. A program takes and returns all parts, laid end to end along the dimension named above; an argument that names none is the same for every part. Nothing has to cross between parts.
All inputs are finite; a program needn't handle non-finite values.
Results may differ from a plain program's by a relative error of at most 0.008.
Values may be sent and summed in bfloat16 or wider, within the bound.
A program may use at most 128 MiB of HBM per device.

v0:
```python
import jax
import jax.numpy as jnp
from jax import lax
from jax.sharding import PartitionSpec as P

HEAD_DIM = 64
WINDOW = 128
GRID_W = 64


def with_halo(cells, sides, width):
    for axis, dim in sides:
        count = lax.axis_size(axis)
        ends = count - 1
        head = lax.slice_in_dim(cells, 0, width, axis=dim)
        tail = lax.slice_in_dim(cells, cells.shape[dim] - width, cells.shape[dim], axis=dim)
        cells = jnp.concatenate(
            [
                lax.ppermute(tail, axis, [(i, (i + 1) % count) for i in range(ends)]),
                cells,
                lax.ppermute(head, axis, [((i + 1) % count, i) for i in range(ends)]),
            ],
            axis=dim,
        )
    return cells


def rotate(values, positions):
    quarter = 16
    inverse = 10000.0 ** (-jnp.arange(quarter, dtype=jnp.float32) / quarter)

    def turn(part, place):
        angle = place.astype(jnp.float32)[:, None] * inverse[None, :]
        cosine = jnp.cos(angle)[:, None, :]
        sine = jnp.sin(angle)[:, None, :]
        first, second = (part[..., :quarter], part[..., quarter:])
        return jnp.concatenate(
            [first * cosine - second * sine, second * cosine + first * sine], axis=-1
        )

    grid_row = positions // GRID_W
    grid_col = positions % GRID_W
    return jnp.concatenate(
        [turn(values[..., :32], grid_row), turn(values[..., 32:], grid_col)], axis=-1
    )


def body(
    resid, queries, keys_values, sink, out_weight, norm_gain, gate_weight, up_weight, down_weight
):
    tok = queries.shape[0]
    heads_here = queries.shape[1] // HEAD_DIM
    kv_here = keys_values.shape[1]
    group = heads_here // kv_here
    cols = resid.shape[1]
    offset = lax.axis_index("sp") * tok
    total_tokens = tok * lax.axis_size("sp")
    positions = offset + jnp.arange(tok, dtype=jnp.int32)
    rotated_q = rotate(
        queries.astype(jnp.float32).reshape(tok, heads_here, HEAD_DIM), positions
    ).astype(jnp.bfloat16)
    rotated_k = rotate(keys_values[..., :HEAD_DIM].astype(jnp.float32), positions).astype(
        jnp.bfloat16
    )
    joined = jnp.concatenate([rotated_k, keys_values[..., HEAD_DIM:]], axis=-1)
    padded = with_halo(joined, (("sp", 0),), WINDOW)
    blocks = tok // WINDOW
    key_blocks = jnp.stack(
        [padded[index * WINDOW : index * WINDOW + 3 * WINDOW] for index in range(blocks)]
    )
    grouped = rotated_q.reshape(blocks, WINDOW, kv_here, group, HEAD_DIM)
    scores = jnp.einsum(
        "nqkgd,njkd->nkgqj", grouped, key_blocks[..., :HEAD_DIM], preferred_element_type=jnp.float32
    ) * HEAD_DIM ** (-0.5)
    block_start = offset + WINDOW * jnp.arange(blocks, dtype=jnp.int32)
    query_pos = block_start[:, None] + jnp.arange(WINDOW, dtype=jnp.int32)[None, :]
    key_pos = block_start[:, None] - WINDOW + jnp.arange(3 * WINDOW, dtype=jnp.int32)[None, :]
    valid = (
        (jnp.abs(query_pos[:, :, None] - key_pos[:, None, :]) <= WINDOW)
        & (key_pos[:, None, :] >= 0)
        & (key_pos[:, None, :] < total_tokens)
    )
    scores = jnp.where(valid[:, None, None], scores, jnp.float32(-1e30))
    sink_grid = sink.reshape(kv_here, group)[None, :, :, None]
    top = jnp.maximum(jnp.max(scores, axis=-1), sink_grid)
    expo = jnp.exp(scores - top[..., None])
    denom = jnp.sum(expo, axis=-1) + jnp.exp(sink_grid - top)
    probs = (expo / denom[..., None]).astype(jnp.bfloat16)
    attended = jnp.einsum(
        "nkgqj,njkd->nqkgd", probs, key_blocks[..., HEAD_DIM:], preferred_element_type=jnp.float32
    )
    attended = attended.astype(jnp.bfloat16).reshape(tok, heads_here * HEAD_DIM)
    attn_rows, resid_rows = (
        lax.all_to_all(attended, "tp", split_axis=0, concat_axis=1, tiled=True),
        lax.all_to_all(resid, "tp", split_axis=0, concat_axis=1, tiled=True),
    )
    whole_out = lax.all_gather(out_weight, "tp", axis=0, tiled=True)
    stream_part = (
        resid_rows.astype(jnp.float32)
        + jnp.dot(attn_rows, whole_out, preferred_element_type=jnp.float32)
    ).astype(jnp.bfloat16)
    stream = lax.all_gather(stream_part, "tp", axis=0, tiled=True)
    stream_cols = lax.dynamic_slice_in_dim(stream, lax.axis_index("tp") * cols, cols, 1)
    widened = stream.astype(jnp.float32)
    normed = (
        widened * lax.rsqrt(jnp.mean(widened * widened, axis=-1, keepdims=True) + 1e-06) * norm_gain
    ).astype(jnp.bfloat16)
    gate = jnp.dot(
        normed,
        lax.all_gather(gate_weight, "sp", axis=0, tiled=True),
        preferred_element_type=jnp.float32,
    )
    up = jnp.dot(
        normed,
        lax.all_gather(up_weight, "sp", axis=0, tiled=True),
        preferred_element_type=jnp.float32,
    )
    hidden = (jax.nn.silu(gate) * up).astype(jnp.bfloat16)
    terms = jnp.dot(
        hidden,
        lax.all_gather(down_weight, "sp", axis=1, tiled=True),
        preferred_element_type=jnp.float32,
    )
    summed = lax.psum_scatter(
        terms.astype(jnp.bfloat16), "tp", scatter_dimension=1, tiled=True
    ).astype(jnp.float32)
    return (stream_cols.astype(jnp.float32) + summed).astype(jnp.bfloat16)


def solution(mesh):
    return jax.shard_map(
        body,
        mesh=mesh,
        in_specs=(
            P(("grp", "sp"), "tp"),
            P(("grp", "sp"), "tp"),
            P(("grp", "sp"), "tp", None),
            P("tp"),
            P("tp", None),
            P(),
            P("sp", "tp"),
            P("sp", "tp"),
            P("tp", "sp"),
        ),
        out_specs=P(("grp", "sp"), "tp"),
        check_vma=False,
    )
```

profile of v0, /device:TPU:0, one launch (start us, length us, event | category | flops | bytes accessed | tf_op | source)
XLA Modules:
  0.0 493.6 jit_solution(14125125992527969314)
XLA Ops:
  7.3 1.7 fusion.49
  9.9 5.0 %collective-permute-start = (bf16[128,2,128]{0,2,1:T(8,128)(2,1)S(1)}, bf16[128,2,128]{0,2,1:T(8,128)(2,1)S(1)}, u32[]{:S(2)}, u32[]{:S(2)}) collective-permute-start(bf16[128,2,128]{0,2,1:T(8,128)(2,1)S(1)} %get-tuple-element.12), channel_id=1, source_target_pairs={{0,4},{4,8},{8,12},{1,5},{5,9},{9,13},{2,6},{6,10},{10,14},{3,7},{... | collective-permute-start | bytes 196616 | tf_op jit(solution)/shard_map/ppermute | solution.py:19
  14.9 1.3 collective-permute-start.1
  16.2 3.5 all-to-all-start
  20.6 1.2 fusion.11
  23.0 1.3 fusion.1
  24.4 1.9 fusion
  26.4 2.3 fusion.9
  28.7 1.6 copy.38
  30.3 1.6 all_to_all.26
  31.9 5.0 %all-to-all-done = bf16[4,160,512]{2,1,0:T(8,128)(2,1)S(1)} async-done(((bf16[4,160,512]{2,1,0:T(8,128)(2,1)}), bf16[4,160,512]{2,1,0:T(8,128)(2,1)S(1)}, u32[]{:S(2)}, u32[]{:S(2)}) %all-to-all-start) | async-done | bytes 655392 | tf_op jit(solution)/shard_map/all_to_all | solution.py:95
  36.9 3.5 all-to-all-start.1
  40.8 17.3 %all-to-all-done.1 = bf16[4,160,512]{2,1,0:T(8,128)(2,1)S(1)} async-done(((bf16[4,160,512]{2,1,0:T(8,128)(2,1)}), bf16[4,160,512]{2,1,0:T(8,128)(2,1)S(1)}, u32[]{:S(2)}, u32[]{:S(2)}) %all-to-all-start.1) | async-done | bytes 655392 | tf_op jit(solution)/shard_map/all_to_all | solution.py:94
  58.1 25.6 %all-gather.6.cloned.1.call-done = bf16[2048,2048]{1,0:T(8,128)(2,1)} async-done(((bf16[512,2048]{1,0:T(8,128)(2,1)}), bf16[2048,2048]{1,0:T(8,128)(2,1)}) %all-gather.6.cloned.1.call-update) | async-done | bytes 8388624 | tf_op jit(solution)/shard_map/all_gather | solution.py:97
  83.7 5.7 %fusion.7 = bf16[160,2048]{1,0:T(8,128)(2,1)} fusion(f32[160,2048]{1,0:T(8,128)S(1)} %bitcast.70, bf16[160,2048]{1,0:T(8,128)(2,1)S(1)} %bitcast.71, bf16[2048,2048]{1,0:T(8,128)(2,1)} %all-gather.6.cloned.1.call-done), kind=kOutput, calls=%fused_computation.15 | convolution fusion | flops 1342832640 | bytes 11010048 | tf_op jit(solution)/shard_map/dot_general | solution.py:100
  91.6 23.8 %all-gather.8.cloned.1.call-done = bf16[640,2048]{1,0:T(8,128)(2,1)} async-done(((bf16[160,2048]{1,0:T(8,128)(2,1)}), bf16[640,2048]{1,0:T(8,128)(2,1)}) %all-gather.8.cloned.1.call-update) | async-done | bytes 2621456 | tf_op jit(solution)/shard_map/all_gather | solution.py:102
  115.4 2.3 fusion.2
  117.8 106.0 %all-gather.10.cloned.1.call-done = bf16[2048,1408]{1,0:T(8,128)(2,1)} async-done(((bf16[512,1408]{1,0:T(8,128)(2,1)}), bf16[2048,1408]{1,0:T(8,128)(2,1)}) %all-gather.10.cloned.1.call-update) | async-done | bytes 5767184 | tf_op jit(solution)/shard_map/all_gather | solution.py:110
  223.7 9.5 %fusion.14 = f32[640,1408]{1,0:T(8,128)} fusion(bf16[2048,1408]{1,0:T(8,128)(2,1)} %all-gather.10.cloned.1.call-done, bf16[640,2048]{1,0:T(8,128)(2,1)} %all-gather.8.cloned.1.call-done, f32[2048]{0:T(1024)S(1)} %copy-done.2, f32[640]{0:T(1024)S(1)} %add_rsqrt_fusion), kind=kOutput, calls=%fused_computation.23 | convolution fusion | flops 3696230400 | bytes 12003840 | tf_op jit(solution)/shard_map/dot_general | solution.py:108
  233.2 96.9 %all-gather.12.cloned.1.call-done = bf16[2048,1408]{1,0:T(8,128)(2,1)} async-done(((bf16[512,1408]{1,0:T(8,128)(2,1)}), bf16[2048,1408]{1,0:T(8,128)(2,1)}) %all-gather.12.cloned.1.call-update) | async-done | bytes 5767184 | tf_op jit(solution)/shard_map/all_gather | solution.py:115
  330.1 106.4 %all-gather.14.cloned.1.call-done = bf16[1408,2048]{1,0:T(8,128)(2,1)} async-done(((bf16[1408,512]{1,0:T(8,128)(2,1)}), bf16[1408,2048]{1,0:T(8,128)(2,1)}) %all-gather.14.cloned.1.call-update) | async-done | bytes 5767184 | tf_op jit(solution)/shard_map/all_gather | solution.py:121
  436.5 15.3 %convolution_convert_fusion = bf16[640,2048]{1,0:T(8,128)(2,1)} fusion(bf16[1408,2048]{1,0:T(8,128)(2,1)} %all-gather.14.cloned.1.call-done, bf16[2048,1408]{1,0:T(8,128)(2,1)} %all-gather.12.cloned.1.call-done, f32[640,1408]{1,0:T(8,128)} %fusion.14, bf16[640,2048]{1,0:T(8,128)(2,1)S(1)} %copy-done, f32[2048]{0:T(1024)S(1)} %copy-done.2, ...), kind=kOutput, calls=%fused_computation.13 | convolution fusion | flops 7393935360 | bytes 20392448 | tf_op jit(solution)/shard_map/dot_general | solution.py:119
  451.9 32.8 %reduce-scatter.2.cloned.1.call-done = bf16[640,512]{1,0:T(8,128)(2,1)} async-done(((bf16[640,2048]{1,0:T(8,128)(2,1)}), bf16[640,512]{1,0:T(8,128)(2,1)}) %reduce-scatter.2.cloned.1.call-update) | async-done | bytes 655376 | tf_op jit(solution)/shard_map/reduce_scatter | solution.py:124
  484.7 2.1 add_convert_fusion
  (61 shorter events, 6.3 us)
Async XLA Ops:
  6.5 13.2 %copy-start.1 = (bf16[640,512]{1,0:T(8,128)(2,1)S(1)}, bf16[640,512]{1,0:T(8,128)(2,1)}, u32[]{:S(2)}) copy-start(bf16[640,512]{1,0:T(8,128)(2,1)} %param.10) | copy-start | bytes 1966084
  6.5 77.1 %all-gather.6.cloned.1.call-start = ((), (), s32[]{:S(2)}) async-start(), calls=%async_computation.3 | async-start | bytes 10485760 | tf_op jit(solution)/shard_map/all_gather | solution.py:97
  9.9 12.9 %collective-permute-start = (bf16[128,2,128]{0,2,1:T(8,128)(2,1)S(1)}, bf16[128,2,128]{0,2,1:T(8,128)(2,1)S(1)}, u32[]{:S(2)}, u32[]{:S(2)}) collective-permute-start(bf16[128,2,128]{0,2,1:T(8,128)(2,1)S(1)} %get-tuple-element.12), channel_id=1, source_target_pairs={{0,4},{4,8},{8,12},{1,5},{5,9},{9,13},{2,6},{6,10},{10,14},{3,7},{... | collective-permute-start | bytes 196616 | tf_op jit(solution)/shard_map/ppermute | solution.py:19
  14.9 8.1 %collective-permute-start.1 = (bf16[128,2,128]{0,2,1:T(8,128)(2,1)S(1)}, bf16[128,2,128]{0,2,1:T(8,128)(2,1)S(1)}, u32[]{:S(2)}, u32[]{:S(2)}) collective-permute-start(bf16[128,2,128]{0,2,1:T(8,128)(2,1)S(1)} %get-tuple-element.11), channel_id=1, source_target_pairs={{4,0},{8,4},{12,8},{5,1},{9,5},{13,9},{6,2},{10,6},{14,10},{7,3},{... | collective-permute-start | bytes 196616 | tf_op jit(solution)/shard_map/ppermute | solution.py:21
  16.2 20.7 %all-to-all-start = ((bf16[4,160,512]{2,1,0:T(8,128)(2,1)}), bf16[4,160,512]{2,1,0:T(8,128)(2,1)S(1)}, u32[]{:S(2)}, u32[]{:S(2)}) async-start(bf16[4,160,512]{2,1,0:T(8,128)(2,1)} %bitcast), calls=%async_computation | async-start | bytes 1310720 | tf_op jit(solution)/shard_map/all_to_all | solution.py:95
  20.0 2.7 copy-start.3
  36.9 21.1 %all-to-all-start.1 = ((bf16[4,160,512]{2,1,0:T(8,128)(2,1)}), bf16[4,160,512]{2,1,0:T(8,128)(2,1)S(1)}, u32[]{:S(2)}, u32[]{:S(2)}) async-start(bf16[4,160,512]{2,1,0:T(8,128)(2,1)} %all_to_all.26), calls=%async_computation.1 | async-start | bytes 1310720 | tf_op jit(solution)/shard_map/all_to_all | solution.py:94
  40.4 75.0 %all-gather.8.cloned.1.call-start = ((), (), s32[]{:S(2)}) async-start(), calls=%async_computation.4 | async-start | bytes 3276800 | tf_op jit(solution)/shard_map/all_gather | solution.py:102
  89.4 134.3 %copy-start.2 = (f32[2048]{0:T(1024)S(1)}, f32[2048]{0:T(1024)}, u32[]{:S(2)}) copy-start(f32[2048]{0:T(1024)} %param.14) | copy-start | bytes 24580
  89.4 134.3 %all-gather.10.cloned.1.call-start = ((), (), s32[]{:S(2)}) async-start(), calls=%async_computation.5 | async-start | bytes 7208960 | tf_op jit(solution)/shard_map/all_gather | solution.py:110
  90.2 239.9 %all-gather.12.cloned.1.call-start = ((), (), s32[]{:S(2)}) async-start(), calls=%async_computation.6 | async-start | bytes 7208960 | tf_op jit(solution)/shard_map/all_gather | solution.py:115
  90.8 345.8 %all-gather.14.cloned.1.call-start = ((), (), s32[]{:S(2)}) async-start(), calls=%async_computation.7 | async-start | bytes 7208960 | tf_op jit(solution)/shard_map/all_gather | solution.py:121
  91.3 393.3 %reduce-scatter.2.cloned.1.call-start = ((), (), s32[]{:S(2)}) async-start(), calls=%async_computation.8 | async-start | bytes 3276800 | tf_op jit(solution)/shard_map/reduce_scatter | solution.py:124
  117.7 318.8 %copy-start = (bf16[640,2048]{1,0:T(8,128)(2,1)S(1)}, bf16[640,2048]{1,0:T(8,128)(2,1)}, u32[]{:S(2)}) copy-start(bf16[640,2048]{1,0:T(8,128)(2,1)} %all-gather.8.cloned.1.call-done) | copy-start | bytes 7864324
Sparse Core Ops, SparseCore 0:
  8.9 74.7 all-gather.5
  89.6 25.8 all-gather.7
  117.0 106.6 all-gather.9
  225.1 104.9 all-gather.11
  331.5 104.9 all-gather.13
  452.0 32.6 reduce-scatter.1
where the time goes:
time: 494 us
  waiting for transfers between devices  416 us (84%)
  matrix products  34.2 us (7%)
  between operations  13.8 us (3%)
  starting transfers between devices  13.6 us (3%)
  other arithmetic  8.95 us (2%)
  local copies, waits for them, and re-layouts  6.91 us (1%)
    all_gather x1, waiting for transfers between devices, body(): lax.all_gather(down_weight, 'sp', axis=1, tiled=True)  106 us
    all_gather x1, waiting for transfers between devices, body(): lax.all_gather(gate_weight, 'sp', axis=0, tiled=True)  106 us
    all_gather x1, waiting for transfers between devices, body(): lax.all_gather(up_weight, 'sp', axis=0, tiled=True)  96.9 us
    reduce_scatter x1, waiting for transfers between devices, body(): lax.psum_scatter(terms.astype(jnp.bfloat16), 'tp', scatter_dimension=1, t...  32.8 us
    all_gather x1, waiting for transfers between devices, body(): whole_out = lax.all_gather(out_weight, 'tp', axis=0, tiled=True)  25.6 us
    all_gather x1, waiting for transfers between devices, body(): stream = lax.all_gather(stream_part, 'tp', axis=0, tiled=True)  23.8 us
    all_to_all x1, waiting for transfers between devices, body(): lax.all_to_all(attended, 'tp', split_axis=0, concat_axis=1, tiled=True)  17.3 us
    dot_general x1, matrix products, body(): jnp.dot(hidden, lax.all_gather(down_weight, 'sp', axis=1, tiled=True), pr...  15.3 us
  transfers between devices with their start and end apart: 10, of which 8 were waited for; matrix products, arithmetic and copies ran while one was open for 5% of the time, Pallas kernels for 0%

commit v1 on v0

--- a/solution.py
+++ b/solution.py
@@ -118,7 +118,7 @@
     hidden = (jax.nn.silu(gate) * up).astype(jnp.bfloat16)
     terms = jnp.dot(
         hidden,
-        lax.all_gather(down_weight, "sp", axis=1, tiled=True),
+        jnp.concatenate(lax.all_gather(down_weight, "sp"), axis=1),
         preferred_element_type=jnp.float32,
     )
     summed = lax.psum_scatter(

time: 494 us -> 490 us (level)
  waiting for transfers between devices: 416 us -> 404 us
  local copies, waits for them, and re-layouts: 6.91 us -> 14.3 us
    reshape x0 -> x1, local copies, waits for them, and re-layouts: none -> 8.42 us  [body(): jnp.concatenate(lax.all_gather(down_weight, 'sp'), axis=1)]
    all_gather x1, waiting for transfers between devices: 23.8 us -> 17 us  [body(): stream = lax.all_gather(stream_part, 'tp', axis=0, tiled=True)]
  transfers between devices with their start and end apart: 10 -> 10, of which waited for: 8 -> 8; matrix products, arithmetic and copies ran while one was open for 5% -> 8% of each run, Pallas kernels for 0% -> 0%
where the time goes in v1:
time: 490 us; the launch traced here: 489 us
  waiting for transfers between devices  404 us (82%)
  matrix products  34.2 us (7%)
  local copies, waits for them, and re-layouts  14.3 us (3%)
  between operations  13.8 us (3%)
  starting transfers between devices  13.6 us (3%)
  other arithmetic  8.98 us (2%)
    all_gather x1, waiting for transfers between devices, body(): lax.all_gather(gate_weight, 'sp', axis=0, tiled=True)  106 us
    all_gather x1, waiting for transfers between devices, body(): lax.all_gather(down_weight, 'sp')  102 us
    all_gather x1, waiting for transfers between devices, body(): lax.all_gather(up_weight, 'sp', axis=0, tiled=True)  96.8 us
    reduce_scatter x1, waiting for transfers between devices, body(): lax.psum_scatter(terms.astype(jnp.bfloat16), 'tp', scatter_dimension=1, t...  32.8 us
    all_gather x1, waiting for transfers between devices, body(): whole_out = lax.all_gather(out_weight, 'tp', axis=0, tiled=True)  25.6 us
    all_to_all x1, waiting for transfers between devices, body(): lax.all_to_all(attended, 'tp', split_axis=0, concat_axis=1, tiled=True)  17.3 us
    all_gather x1, waiting for transfers between devices, body(): stream = lax.all_gather(stream_part, 'tp', axis=0, tiled=True)  17 us
    dot_general x1, matrix products, body(): jnp.dot(hidden, jnp.concatenate(lax.all_gather(down_weight, 'sp'), axis=1...  15.3 us
  transfers between devices with their start and end apart: 10, of which 8 were waited for; matrix products, arithmetic and copies ran while one was open for 8% of the time, Pallas kernels for 0%

profile of v1, /device:TPU:0, one launch (start us, length us, event | category | flops | bytes accessed | tf_op | source)
XLA Modules:
  0.0 489.2 jit_solution(13088630771603515031)
XLA Ops:
  9.6 5.0 %collective-permute-start = (bf16[128,2,128]{0,2,1:T(8,128)(2,1)S(1)}, bf16[128,2,128]{0,2,1:T(8,128)(2,1)S(1)}, u32[]{:S(2)}, u32[]{:S(2)}) collective-permute-start(bf16[128,2,128]{0,2,1:T(8,128)(2,1)S(1)} %get-tuple-element.12), channel_id=1, source_target_pairs={{0,4},{4,8},{8,12},{1,5},{5,9},{9,13},{2,6},{6,10},{10,14},{3,7},{... | collective-permute-start | bytes 196616 | tf_op jit(solution)/shard_map/ppermute | solution.py:19
  14.6 1.3 collective-permute-start.1
  15.9 3.5 all-to-all-start
  20.3 1.2 fusion.11
  22.7 1.3 fusion.1
  24.1 1.9 fusion
  26.1 2.3 fusion.9
  28.4 1.6 copy.50
  30.1 1.6 all_to_all.26
  31.7 4.9 all-to-all-done
  36.6 3.5 all-to-all-start.1
  40.4 17.3 %all-to-all-done.1 = bf16[4,160,512]{2,1,0:T(8,128)(2,1)S(1)} async-done(((bf16[4,160,512]{2,1,0:T(8,128)(2,1)}), bf16[4,160,512]{2,1,0:T(8,128)(2,1)S(1)}, u32[]{:S(2)}, u32[]{:S(2)}) %all-to-all-start.1) | async-done | bytes 655392 | tf_op jit(solution)/shard_map/all_to_all | solution.py:94
  57.8 25.6 %all-gather.7.cloned.1.call-done = bf16[2048,2048]{1,0:T(8,128)(2,1)} async-done(((bf16[512,2048]{1,0:T(8,128)(2,1)}), bf16[2048,2048]{1,0:T(8,128)(2,1)}) %all-gather.7.cloned.1.call-update) | async-done | bytes 8388624 | tf_op jit(solution)/shard_map/all_gather | solution.py:97
  83.4 5.8 %fusion.7 = bf16[160,2048]{1,0:T(8,128)(2,1)} fusion(f32[160,2048]{1,0:T(8,128)S(1)} %bitcast.76, bf16[160,2048]{1,0:T(8,128)(2,1)S(1)} %bitcast.77, bf16[2048,2048]{1,0:T(8,128)(2,1)} %all-gather.7.cloned.1.call-done), kind=kOutput, calls=%fused_computation.15 | convolution fusion | flops 1342832640 | bytes 11010048 | tf_op jit(solution)/shard_map/dot_general | solution.py:100
  90.5 101.7 %all-gather.15.cloned.1.call-done = bf16[5632,512]{1,0:T(8,128)(2,1)} async-done(((bf16[1408,512]{1,0:T(8,128)(2,1)}), bf16[5632,512]{1,0:T(8,128)(2,1)}) %all-gather.15.cloned.1.call-update) | async-done | bytes 5767184 | tf_op jit(solution)/shard_map/all_gather | solution.py:121
  192.2 8.4 %copy.52 = bf16[1408,4,512]{0,2,1:T(8,128)(2,1)} copy(bf16[1408,4,512]{2,0,1:T(8,128)(2,1)} %bitcast.74) | data formatting | bytes 11534336 | tf_op jit(solution)/shard_map/reshape | solution.py:121
  200.7 17.0 %all-gather.9.cloned.1.call-done = bf16[640,2048]{1,0:T(8,128)(2,1)} async-done(((bf16[160,2048]{1,0:T(8,128)(2,1)}), bf16[640,2048]{1,0:T(8,128)(2,1)}) %all-gather.9.cloned.1.call-update) | async-done | bytes 2621456 | tf_op jit(solution)/shard_map/all_gather | solution.py:102
  217.6 2.3 fusion.2
  220.0 105.8 %all-gather.11.cloned.1.call-done = bf16[2048,1408]{1,0:T(8,128)(2,1)} async-done(((bf16[512,1408]{1,0:T(8,128)(2,1)}), bf16[2048,1408]{1,0:T(8,128)(2,1)}) %all-gather.11.cloned.1.call-update) | async-done | bytes 5767184 | tf_op jit(solution)/shard_map/all_gather | solution.py:110
  325.8 9.6 %fusion.14 = f32[640,1408]{1,0:T(8,128)} fusion(bf16[2048,1408]{1,0:T(8,128)(2,1)} %all-gather.11.cloned.1.call-done, bf16[640,2048]{1,0:T(8,128)(2,1)} %all-gather.9.cloned.1.call-done, f32[2048]{0:T(1024)S(1)} %copy-done.3, f32[640]{0:T(1024)S(1)} %add_rsqrt_fusion), kind=kOutput, calls=%fused_computation.23 | convolution fusion | flops 3696230400 | bytes 12003840 | tf_op jit(solution)/shard_map/dot_general | solution.py:108
  335.3 96.8 %all-gather.13.cloned.1.call-done = bf16[2048,1408]{1,0:T(8,128)(2,1)} async-done(((bf16[512,1408]{1,0:T(8,128)(2,1)}), bf16[2048,1408]{1,0:T(8,128)(2,1)}) %all-gather.13.cloned.1.call-update) | async-done | bytes 5767184 | tf_op jit(solution)/shard_map/all_gather | solution.py:115
  432.2 15.3 %convolution_convert_fusion = bf16[640,2048]{1,0:T(8,128)(2,1)} fusion(bf16[1408,2048]{0,1:T(8,128)(2,1)} %bitcast.75, bf16[2048,1408]{1,0:T(8,128)(2,1)} %all-gather.13.cloned.1.call-done, f32[640,1408]{1,0:T(8,128)} %fusion.14, bf16[640,2048]{1,0:T(8,128)(2,1)S(1)} %copy-done, f32[2048]{0:T(1024)S(1)} %copy-done.3, f32[640]{0:T(1024)S(1)} %add_rsqrt_fusion), kind=kOutput, calls=%fused_computation.13 | convolution fusion | flops 7393935360 | bytes 20392448 | tf_op jit(solution)/shard_map/dot_general | solution.py:119
  447.5 32.8 %reduce-scatter.2.cloned.1.call-done = bf16[640,512]{1,0:T(8,128)(2,1)} async-done(((bf16[640,2048]{1,0:T(8,128)(2,1)}), bf16[640,512]{1,0:T(8,128)(2,1)}) %reduce-scatter.2.cloned.1.call-update) | async-done | bytes 655376 | tf_op jit(solution)/shard_map/reduce_scatter | solution.py:124
  480.2 2.1 add_convert_fusion
  (64 shorter events, 6.9 us)
Async XLA Ops:
  6.5 1.5 copy-start.1
  6.5 76.8 %all-gather.7.cloned.1.call-start = ((), (), s32[]{:S(2)}) async-start(), calls=%async_computation.3 | async-start | bytes 10485760 | tf_op jit(solution)/shard_map/all_gather | solution.py:97
  7.3 12.2 %copy-start.2 = (bf16[640,512]{1,0:T(8,128)(2,1)S(1)}, bf16[640,512]{1,0:T(8,128)(2,1)}, u32[]{:S(2)}) copy-start(bf16[640,512]{1,0:T(8,128)(2,1)} %param.10) | copy-start | bytes 1966084
  7.3 185.0 %all-gather.15.cloned.1.call-start = ((), (), s32[]{:S(2)}) async-start(), calls=%async_computation.8 | async-start | bytes 7208960 | tf_op jit(solution)/shard_map/all_gather | solution.py:121
  9.6 12.9 %collective-permute-start = (bf16[128,2,128]{0,2,1:T(8,128)(2,1)S(1)}, bf16[128,2,128]{0,2,1:T(8,128)(2,1)S(1)}, u32[]{:S(2)}, u32[]{:S(2)}) collective-permute-start(bf16[128,2,128]{0,2,1:T(8,128)(2,1)S(1)} %get-tuple-element.12), channel_id=1, source_target_pairs={{0,4},{4,8},{8,12},{1,5},{5,9},{9,13},{2,6},{6,10},{10,14},{3,7},{... | collective-permute-start | bytes 196616 | tf_op jit(solution)/shard_map/ppermute | solution.py:19
  14.6 8.1 %collective-permute-start.1 = (bf16[128,2,128]{0,2,1:T(8,128)(2,1)S(1)}, bf16[128,2,128]{0,2,1:T(8,128)(2,1)S(1)}, u32[]{:S(2)}, u32[]{:S(2)}) collective-permute-start(bf16[128,2,128]{0,2,1:T(8,128)(2,1)S(1)} %get-tuple-element.11), channel_id=1, source_target_pairs={{4,0},{8,4},{12,8},{5,1},{9,5},{13,9},{6,2},{10,6},{14,10},{7,3},{... | collective-permute-start | bytes 196616 | tf_op jit(solution)/shard_map/ppermute | solution.py:21
  15.9 20.7 %all-to-all-start = ((bf16[4,160,512]{2,1,0:T(8,128)(2,1)}), bf16[4,160,512]{2,1,0:T(8,128)(2,1)S(1)}, u32[]{:S(2)}, u32[]{:S(2)}) async-start(bf16[4,160,512]{2,1,0:T(8,128)(2,1)} %bitcast), calls=%async_computation | async-start | bytes 1310720 | tf_op jit(solution)/shard_map/all_to_all | solution.py:95
  19.7 2.7 copy-start.4
  36.6 21.1 %all-to-all-start.1 = ((bf16[4,160,512]{2,1,0:T(8,128)(2,1)}), bf16[4,160,512]{2,1,0:T(8,128)(2,1)S(1)}, u32[]{:S(2)}, u32[]{:S(2)}) async-start(bf16[4,160,512]{2,1,0:T(8,128)(2,1)} %all_to_all.26), calls=%async_computation.1 | async-start | bytes 1310720 | tf_op jit(solution)/shard_map/all_to_all | solution.py:94
  40.1 177.6 %all-gather.9.cloned.1.call-start = ((), (), s32[]{:S(2)}) async-start(), calls=%async_computation.4 | async-start | bytes 3276800 | tf_op jit(solution)/shard_map/all_gather | solution.py:102
  89.1 236.6 %all-gather.11.cloned.1.call-start = ((), (), s32[]{:S(2)}) async-start(), calls=%async_computation.5 | async-start | bytes 7208960 | tf_op jit(solution)/shard_map/all_gather | solution.py:110
  89.7 342.4 %all-gather.13.cloned.1.call-start = ((), (), s32[]{:S(2)}) async-start(), calls=%async_computation.6 | async-start | bytes 7208960 | tf_op jit(solution)/shard_map/all_gather | solution.py:115
  90.3 389.9 %reduce-scatter.2.cloned.1.call-start = ((), (), s32[]{:S(2)}) async-start(), calls=%async_computation.7 | async-start | bytes 3276800 | tf_op jit(solution)/shard_map/reduce_scatter | solution.py:124
  192.2 133.5 %copy-start.3 = (f32[2048]{0:T(1024)S(1)}, f32[2048]{0:T(1024)}, u32[]{:S(2)}) copy-start(f32[2048]{0:T(1024)} %param.14) | copy-start | bytes 24580
  220.0 212.2 %copy-start = (bf16[640,2048]{1,0:T(8,128)(2,1)S(1)}, bf16[640,2048]{1,0:T(8,128)(2,1)}, u32[]{:S(2)}) copy-start(bf16[640,2048]{1,0:T(8,128)(2,1)} %all-gather.9.cloned.1.call-done) | copy-start | bytes 7864324
Sparse Core Ops, SparseCore 0:
  8.9 74.4 all-gather.6
  84.9 107.2 all-gather.14
  193.8 23.7 all-gather.8
  219.1 106.6 all-gather.10
  327.2 104.9 all-gather.12
  447.6 32.6 reduce-scatter.1
